TPU v7x, 32 devices: a whole 2x2x4 slice. The times are simulated.
32 devices in a mesh: kv: 8 (over z, x), tp: 4 (over y, core).
Axes of the slice: x: 2, y: 2, z: 4, core: 2. Of those that a mesh axis runs over, the one named last changes fastest.
Arguments:
- tokens: bfloat16 [384, 4096], P(None, ('kv', 'tp')), may hold values from -90 to 90
- norm_gain: float32 [4096], P('kv'), may hold values from 0.1 to 1.9
- w_query: bfloat16 [4096, 2048], P('kv', 'tp'), may hold values from -0.09375 to 0.09375
- w_key: bfloat16 [4096, 2048], P('kv', 'tp'), may hold values from -0.09375 to 0.09375
- w_value: bfloat16 [4096, 2048], P('kv', 'tp'), may hold values from -0.09375 to 0.09375
- w_outgate: bfloat16 [4096, 2048], P('kv', 'tp'), may hold values from -0.09375 to 0.09375
- w_igate: bfloat16 [4096, 16], replicated, may hold values from -0.09375 to 0.09375
- w_fgate: bfloat16 [4096, 16], replicated, may hold values from -0.09375 to 0.09375
- forget_bias: float32 [16], P('tp'), may hold values from -1 to 5
- head_gain: float32 [2048], P('tp'), may hold values from 0.1 to 1.9
- w_proj: bfloat16 [2048, 4096], P('tp', 'kv'), may hold values from -0.125 to 0.125
- mixer_gain: float32 [4096], P('kv'), may hold values from 0.1 to 1.9
- w_gate: bfloat16 [4096, 11264], P('kv', 'tp'), may hold values from -0.09375 to 0.09375
- w_up: bfloat16 [4096, 11264], P('kv', 'tp'), may hold values from -0.09375 to 0.09375
- w_down: bfloat16 [11264, 4096], P('tp', 'kv'), may hold values from -0.0546875 to 0.0546875
- state_c: float32 [384, 16, 128, 128], P('kv', 'tp'), may hold values from -0.5 to 0.5
- state_m: float32 [384, 16], P('kv', 'tp'), may hold values from -4 to 4
- tail_keys: bfloat16 [384, 16, 64, 128], P('kv', 'tp'), may hold values from -6 to 6
- tail_values: bfloat16 [384, 16, 64, 128], P('kv', 'tp'), may hold values from -6 to 6
- tail_gate: float32 [384, 16, 64], P('kv', 'tp'), may hold values from -8 to 130
- block_forget: float32 [384, 16], P('kv', 'tp'), may hold values from -6 to 0
- lengths: int32 [384], P('kv'), may hold values from 1 to 64, 6144 in all
Outputs:
- result: bfloat16 [384, 4096], P(None, ('kv', 'tp'))
All inputs are finite; a program needn't handle non-finite values. No bound on the sum of `lengths` on one device may be relied on, other than what follows from the above.
Results may differ from a plain program's by a relative error of at most 0.012.
Values may be sent and summed in bfloat16 or wider, within the bound.
A program may use at most 128 MiB of HBM per device.

v0:
```python
import jax
import jax.numpy as jnp
from jax import lax
from jax.sharding import PartitionSpec as P

D = 4096


EPS = 1e-06


def recall(
    query,
    key,
    value,
    igate,
    fpre,
    state_c,
    state_m,
    tail_keys,
    tail_values,
    tail_gate,
    block_forget,
    lengths,
):
    f32 = jnp.float32
    span = tail_keys.shape[2]
    head_dim = query.shape[2]
    running = block_forget + jax.nn.log_sigmoid(fpre)
    inter = running + state_m
    live = jnp.arange(span, dtype=jnp.int32)[None, :] < lengths[:, None]
    tail_log = jnp.where(live[:, None, :], running[:, :, None] + tail_gate, -jnp.inf)
    top = jnp.maximum(jnp.maximum(inter, jnp.max(tail_log, axis=2)), igate)
    w_inter = jnp.exp(inter - top)
    w_tail = jnp.exp(tail_log - top[:, :, None])
    w_own = jnp.exp(igate - top)
    scores = jnp.einsum("shpd,shd->shp", tail_keys.astype(f32), query) * head_dim ** (-0.5)
    own = jnp.sum(query * key, axis=2)
    memory = jnp.einsum("shvk,shk->shv", state_c, query)
    weighted = w_tail * scores
    return (
        w_inter[:, :, None] * memory
        + jnp.einsum("shp,shpv->shv", weighted, tail_values.astype(f32))
        + (w_own * own)[:, :, None] * value
    )


def per_device(
    tokens,
    norm_gain,
    w_query,
    w_key,
    w_value,
    w_outgate,
    w_igate,
    w_fgate,
    forget_bias,
    head_gain,
    w_proj,
    mixer_gain,
    w_gate,
    w_up,
    w_down,
    state_c,
    state_m,
    tail_keys,
    tail_values,
    tail_gate,
    block_forget,
    lengths,
):
    f32 = jnp.float32
    bf = jnp.bfloat16
    kv_pos = lax.axis_index("kv")
    tp_pos = lax.axis_index("tp")
    rows = norm_gain.shape[0]
    heads = forget_bias.shape[0]
    head_dim = tail_keys.shape[3]
    seq_dev = lengths.shape[0]
    width = heads * head_dim
    wide = lax.all_gather(tokens, "tp", axis=1, tiled=True)
    widef = wide.astype(f32)
    scaled = (widef * norm_gain).astype(bf)

    def local_cols(weight):
        return lax.dynamic_slice(weight, (kv_pos * rows, tp_pos * heads), (rows, heads))

    gate_weights = jnp.concatenate([local_cols(w_igate), local_cols(w_fgate)], axis=1)
    joined = jnp.concatenate([w_query, w_key, w_value, w_outgate], axis=1)
    proj = jnp.dot(scaled, joined, preferred_element_type=f32)
    gates = jnp.dot(scaled, gate_weights, preferred_element_type=f32)
    tokf = tokens.astype(f32)
    sq_all = lax.psum(jnp.sum(tokf * tokf, axis=1), ("kv", "tp"))
    proj, gates = (
        lax.psum_scatter(proj, "kv", scatter_dimension=0, tiled=True),
        lax.psum_scatter(gates, "kv", scatter_dimension=0, tiled=True),
    )
    inv_first = lax.dynamic_slice_in_dim(lax.rsqrt(sq_all / D + EPS), kv_pos * seq_dev, seq_dev)
    proj = proj * inv_first[:, None]
    gates = gates * inv_first[:, None]
    query = proj[:, :width].reshape(seq_dev, heads, head_dim)
    key = proj[:, width : 2 * width].reshape(seq_dev, heads, head_dim) * head_dim ** (-0.5)
    value = proj[:, 2 * width : 3 * width].reshape(seq_dev, heads, head_dim)
    outgate = proj[:, 3 * width :]
    igate = gates[:, :heads]
    fpre = gates[:, heads:] + forget_bias
    recalled = recall(
        query,
        key,
        value,
        igate,
        fpre,
        state_c,
        state_m,
        tail_keys,
        tail_values,
        tail_gate,
        block_forget,
        lengths,
    )
    normed = recalled * lax.rsqrt(jnp.mean(recalled * recalled, axis=2, keepdims=True) + EPS)
    mixed = (normed.reshape(seq_dev, width) * head_gain * jax.nn.sigmoid(outgate)).astype(bf)
    partial_value = jnp.dot(
        lax.all_gather(mixed, "kv", axis=0, tiled=True), w_proj, preferred_element_type=f32
    )
    attended = lax.psum(partial_value.astype(jnp.bfloat16), "tp").astype(jnp.float32)
    middle = (widef + attended).astype(bf)
    middlef = middle.astype(f32)
    part_sq2 = jnp.sum(middlef * middlef, axis=1)
    scaled_mid = (middlef * mixer_gain).astype(bf)
    gate_part = jnp.dot(scaled_mid, w_gate, preferred_element_type=f32)
    up_part = jnp.dot(scaled_mid, w_up, preferred_element_type=f32)
    gate_sh, up_sh, sq_sh = (
        lax.psum_scatter(gate_part, "kv", scatter_dimension=0, tiled=True),
        lax.psum_scatter(up_part, "kv", scatter_dimension=0, tiled=True),
        lax.psum_scatter(part_sq2, "kv", scatter_dimension=0, tiled=True),
    )
    inv_second = lax.rsqrt(sq_sh / D + EPS)[:, None]
    hidden_sh = (jax.nn.silu(gate_sh * inv_second) * (up_sh * inv_second)).astype(bf)
    down_part = jnp.dot(
        lax.all_gather(hidden_sh, "kv", axis=0, tiled=True), w_down, preferred_element_type=f32
    )
    down_sum = lax.psum_scatter(
        down_part.astype(jnp.bfloat16), "tp", scatter_dimension=1, tiled=True
    ).astype(jnp.float32)
    columns = down_sum.shape[1]
    residual = lax.dynamic_slice_in_dim(middlef, tp_pos * columns, columns, 1)
    return (residual + down_sum).astype(bf)


def solution(mesh):
    return jax.shard_map(
        per_device,
        mesh=mesh,
        in_specs=(
            P(None, ("kv", "tp")),
            P("kv"),
            P("kv", "tp"),
            P("kv", "tp"),
            P("kv", "tp"),
            P("kv", "tp"),
            P(),
            P(),
            P("tp"),
            P("tp"),
            P("tp", "kv"),
            P("kv"),
            P("kv", "tp"),
            P("kv", "tp"),
            P("tp", "kv"),
            P("kv", "tp", None, None),
            P("kv", "tp"),
            P("kv", "tp", None, None),
            P("kv", "tp", None, None),
            P("kv", "tp", None),
            P("kv", "tp"),
            P("kv"),
        ),
        out_specs=P(None, ("kv", "tp")),
        check_vma=False,
    )
```

profile of v0, /device:TPU:0, one launch (start us, length us, event | category | flops | bytes accessed | tf_op | source)
XLA Modules:
  0.0 528.5 jit_solution(12030437930786760978)
XLA Ops:
  6.5 0.9 dynamic_slice.12
  7.5 0.8 dynamic_slice.13
  8.3 8.2 %all_gather.9 = bf16[384,512]{1,0:T(8,128)(2,1)S(1)} all-gather(bf16[384,128]{1,0:T(8,128)(2,1)} %param.22), channel_id=1, replica_groups=mesh['kv'=8,'tp'=4] {'tp'}, dimensions={1}, use_global_device_ids=true | all-gather | bytes 491520 | tf_op jit(solution)/shard_map/all_gather | solution.py:81
  16.5 1.6 fusion.12
  18.1 4.2 fusion
  22.4 1.0 multiply_reduce_fusion.1
  23.4 40.2 %psum.14 = f32[384]{0:T(512)S(1)} all-reduce(f32[384]{0:T(512)S(1)} %multiply_reduce_fusion.1), channel_id=1, replica_groups=mesh['kv'=8,'tp'=4] {'kv','tp'}, use_global_device_ids=true, to_apply=%region_2.0 | all-reduce | flops 384 | bytes 3072 | tf_op jit(solution)/shard_map/psum | solution.py:93
  64.3 16.8 %reduce-scatter.16.cloned.1.call-done = f32[48,8]{1,0:T(8,128)} async-done(((f32[384,8]{1,0:T(8,128)}), f32[48,8]{1,0:T(8,128)}) %reduce-scatter.16.cloned.1.call-update) | async-done | bytes 1552
  81.1 0.8 copy.51
  82.5 1.4 fusion.33
  84.5 1.7 fusion.21
  86.2 1.4 copy.38
  87.6 1.3 subtract_exponential_fusion
  88.9 0.7 copy.40
  89.6 1.4 copy.39
  91.0 67.4 %reduce-scatter.10.cloned.1.call-done = f32[48,2048]{1,0:T(8,128)} async-done(((f32[384,2048]{1,0:T(8,128)}), f32[48,2048]{1,0:T(8,128)}) %reduce-scatter.10.cloned.1.call-update) | async-done | bytes 393232 | tf_op jit(solution)/shard_map/reduce_scatter | solution.py:95
  158.4 1.1 broadcast_multiply_fusion
  159.5 0.7 copy-done.1
  160.2 0.7 slice_multiply_fusion
  160.9 1.6 reshape.50
  162.5 1.5 reshape.47
  164.0 1.6 mul.152
  165.6 1.7 multiply_reduce_fusion.3
  167.3 1.4 copy.41
  168.7 1.3 exponential_multiply_fusion
  169.9 1.4 copy.42
  171.3 4.3 fusion.36
  175.7 8.6 %fusion.35 = f32[48,4,1,128]{3,2,1,0:T(1,128)} fusion(f32[48,4,128,1]{2,3,1,0:T(1,128)S(1)} %bitcast.36, f32[48,4,128,128]{3,2,1,0:T(8,128)} %param.37), kind=kOutput, calls=%fused_computation.58 | convolution fusion | flops 6291456 | bytes 12779520 | tf_op jit(solution)/shard_map/shvk,shk->shv/dot_general | solution.py:39
  184.2 1.6 reshape.48
  185.8 1.2 multiply_multiply_fusion
  187.0 0.9 fusion.37
  188.4 0.9 fusion.17
  189.3 31.0 %all_gather.10 = bf16[384,512]{1,0:T(8,128)(2,1)S(1)} all-gather(bf16[48,512]{1,0:T(8,128)(2,1)S(1)} %fusion.17), channel_id=1, replica_groups=mesh['kv'=8,'tp'=4] {'kv'}, dimensions={0}, use_global_device_ids=true | all-gather | bytes 442368 | tf_op jit(solution)/shard_map/all_gather | solution.py:124
  220.3 1.1 convolution_convert_fusion.1
  221.5 32.0 %all-reduce.3.cloned.1.call-done = bf16[384,512]{1,0:T(8,128)(2,1)} async-done(((bf16[384,512]{1,0:T(8,128)(2,1)}), bf16[384,512]{1,0:T(8,128)(2,1)}) %all-reduce.3.cloned.1.call-update) | async-done | bytes 393232 | tf_op jit(solution)/shard_map/psum | solution.py:126
  253.5 5.2 fusion.15
  258.8 5.3 fusion.14
  265.9 2.1 fusion.10
  268.0 22.5 %all-reduce = f32[384]{0:T(512)S(1)} all-reduce(f32[384]{0:T(512)S(1)} %get-tuple-element.12), channel_id=5, replica_groups=mesh['kv'=8,'tp'=4] {'kv'}, use_global_device_ids=true, to_apply=%region_10.11.clone | all-reduce | flops 384 | bytes 3072
  290.6 59.3 %reduce-scatter.12.cloned.1.call-done = f32[48,2816]{1,0:T(8,128)} async-done(((f32[384,2816]{1,0:T(8,128)}), f32[48,2816]{1,0:T(8,128)}) %reduce-scatter.12.cloned.1.call-update) | async-done | bytes 540688 | tf_op jit(solution)/shard_map/reduce_scatter | solution.py:134
  349.8 93.3 %reduce-scatter.14.cloned.1.call-done = f32[48,2816]{1,0:T(8,128)} async-done(((f32[384,2816]{1,0:T(8,128)}), f32[48,2816]{1,0:T(8,128)}) %reduce-scatter.14.cloned.1.call-update) | async-done | bytes 540688 | tf_op jit(solution)/shard_map/reduce_scatter | solution.py:135
  443.1 2.2 multiply_convert_fusion.1
  445.4 49.5 %all-gather.2.cloned.1.call-done = bf16[384,2816]{1,0:T(8,128)(2,1)} async-done(((bf16[48,2816]{1,0:T(8,128)(2,1)}), bf16[384,2816]{1,0:T(8,128)(2,1)}) %all-gather.2.cloned.1.call-update) | async-done | bytes 2162704 | tf_op jit(solution)/shard_map/all_gather | solution.py:141
  494.9 3.7 convolution_convert_fusion
  498.7 0.9 copy.52
  499.6 19.5 %reduce-scatter.18.cloned.1.call-done = bf16[128,384]{1,0:T(8,128)(2,1)} async-done(((bf16[512,384]{1,0:T(8,128)(2,1)}), bf16[128,384]{1,0:T(8,128)(2,1)}) %reduce-scatter.18.cloned.1.call-update) | async-done | bytes 98320
  519.1 1.0 copy.53
  520.1 1.6 add_convert_fusion
  (47 shorter events, 3.9 us)
Async XLA Ops:
  6.5 180.5 %copy-start = (bf16[48,4,64,128]{3,2,1,0:T(8,128)(2,1)S(1)}, bf16[48,4,64,128]{3,2,1,0:T(8,128)(2,1)}, u32[]{:S(2)}) copy-start(bf16[48,4,64,128]{3,2,1,0:T(8,128)(2,1)} %param.40) | copy-start | bytes 9437188
  6.5 74.6 %reduce-scatter.16.cloned.1.call-start = ((), (), s32[]{:S(2)}) async-start(), calls=%async_computation.10 | async-start | bytes 221184
  18.1 140.3 %reduce-scatter.10.cloned.1.call-start = ((), (), s32[]{:S(2)}) async-start(), calls=%async_computation.5 | async-start | bytes 3538944 | tf_op jit(solution)/shard_map/reduce_scatter | solution.py:95
  22.3 41.9 %copy-start.10 = (s32[48]{0:T(128)S(1)}, s32[48]{0:T(128)}, u32[]{:S(2)}) copy-start(s32[48]{0:T(128)} %param.43) | copy-start | bytes 580
  22.3 231.1 %all-reduce.3.cloned.1.call-start = ((), (), s32[]{:S(2)}) async-start(), calls=%async_computation.6 | async-start | bytes 786432 | tf_op jit(solution)/shard_map/psum | solution.py:126
  159.5 0.7 copy-start.1
  171.3 4.3 copy-start.4
  184.2 4.2 copy-start.9
  185.8 2.2 copy-start.3
  185.8 2.2 copy-start.5
  185.8 2.2 copy-start.6
  185.8 2.2 copy-start.7
  185.8 34.5 %copy-start.2 = (bf16[512,512]{1,0:T(8,128)(2,1)S(1)}, bf16[512,512]{1,0:T(8,128)(2,1)}, u32[]{:S(2)}) copy-start(bf16[512,512]{1,0:T(8,128)(2,1)} %param.32) | copy-start | bytes 1572868
  187.0 66.4 %copy-start.8 = (f32[512]{0:T(512)S(1)}, f32[512]{0:T(512)}, u32[]{:S(2)}) copy-start(f32[512]{0:T(512)} %param.33) | copy-start | bytes 6148
  221.4 128.4 %reduce-scatter.12.cloned.1.call-start = ((), (), s32[]{:S(2)}) async-start(), calls=%async_computation.7 | async-start | bytes 4866048 | tf_op jit(solution)/shard_map/reduce_scatter | solution.py:134
  258.7 184.4 %reduce-scatter.14.cloned.1.call-start = ((), (), s32[]{:S(2)}) async-start(), calls=%async_computation.8 | async-start | bytes 4866048 | tf_op jit(solution)/shard_map/reduce_scatter | solution.py:135
  264.0 0.7 copy-start.11
  264.0 230.9 %all-gather.2.cloned.1.call-start = ((), (), s32[]{:S(2)}) async-start(), calls=%async_computation.9 | async-start | bytes 2433024 | tf_op jit(solution)/shard_map/all_gather | solution.py:141
  445.3 73.8 %reduce-scatter.18.cloned.1.call-start = ((), (), s32[]{:S(2)}) async-start(), calls=%async_computation.11 | async-start | bytes 491520
Sparse Core Ops, SparseCore 0:
  18.2 62.8 reduce-scatter.15
  84.7 73.6 reduce-scatter.9
  221.6 31.8 all-reduce.2
  258.8 90.9 reduce-scatter.11
  353.3 89.8 reduce-scatter.13
  445.5 49.4 all-gather.1
  499.7 19.3 reduce-scatter.17
where the time goes:
time: 530 us; the launch traced here: 529 us
  waiting for transfers between devices  338 us (64%)
  blocking collectives  102 us (19%)
  matrix products  34.9 us (7%)
  local copies, waits for them, and re-layouts  20.1 us (4%)
  other arithmetic  19.2 us (4%)
  between operations  14.3 us (3%)
    reduce_scatter x1, waiting for transfers between devices, per_device(): lax.psum_scatter(up_part, 'kv', scatter_dimension=0, tiled=True)  93.3 us
    reduce_scatter x1, waiting for transfers between devices, per_device(): lax.psum_scatter(proj, 'kv', scatter_dimension=0, tiled=True)  67.4 us
    reduce_scatter x1, waiting for transfers between devices, per_device(): lax.psum_scatter(gate_part, 'kv', scatter_dimension=0, tiled=True)  59.3 us
    all_gather x1, waiting for transfers between devices, per_device(): lax.all_gather(hidden_sh, 'kv', axis=0, tiled=True)  49.5 us
    psum x1, blocking collectives, per_device(): sq_all = lax.psum(jnp.sum(tokf * tokf, axis=1), ('kv', 'tp'))  40.2 us
    unnamed x9, waiting for transfers between devices  36.4 us
    psum x1, waiting for transfers between devices, per_device(): lax.psum(partial_value.astype(jnp.bfloat16), 'tp').astype(jnp.float32)  32 us
    all_gather x1, blocking collectives, per_device(): lax.all_gather(mixed, 'kv', axis=0, tiled=True)  31 us
  transfers between devices with their start and end apart: 7, of which 7 were waited for; matrix products, arithmetic and copies ran while one was open for 4% of the time, Pallas kernels for 0%

commit v1 on v0

--- a/solution.py
+++ b/solution.py
@@ -1,7 +1,279 @@
+import functools
+
 import jax
 import jax.numpy as jnp
 from jax import lax
+from jax.experimental import pallas as pl
+from jax.experimental.pallas import tpu as pltpu
 from jax.sharding import PartitionSpec as P
+
+MESH = pl.DeviceIdType.MESH
+
+
+def flip(pos, mask):
+    out, bit = pos, 1
+    while bit <= mask:
+        if mask & bit:
+            out = out + bit - 2 * bit * lax.rem(lax.div(pos, bit), 2)
+        bit *= 2
+    return out
+
+
+def meet(axis, peers):
+    barrier = pltpu.get_barrier_semaphore()
+    for peer in peers:
+        pl.semaphore_signal(barrier, inc=1, device_id={axis: peer}, device_id_type=MESH)
+    pl.semaphore_wait(barrier, len(peers))
+
+
+def send(src, dst, send_sem, recv_sem, axis, peer):
+    copy = pltpu.make_async_remote_copy(
+        src_ref=src,
+        dst_ref=dst,
+        send_sem=send_sem,
+        recv_sem=recv_sem,
+        device_id={axis: peer},
+        device_id_type=MESH,
+    )
+    copy.start()
+    return copy
+
+
+def scatter_kernel(axis, outer, inner, jobs, count, *refs):
+    f32 = jnp.float32
+    ins, outs = refs[:count], refs[count : 2 * count]
+    refs = refs[2 * count :]
+    if inner > 1:
+        recv1, refs = refs[:count], refs[count:]
+        mid, refs = refs[:count], refs[count:]
+    recv2, refs = refs[:count], refs[count:]
+    if inner > 1:
+        send1_sem, recv1_sem = refs[:2]
+        refs = refs[2:]
+    send2_sem, recv2_sem = refs
+    me = lax.axis_index(axis)
+    my_out, my_in = lax.div(me, inner), lax.rem(me, inner)
+    in_peers = [flip(my_in, d) for d in range(1, inner)]
+    out_peers = [flip(my_out, d) for d in range(1, outer)]
+    meet(
+        axis,
+        [my_out * inner + p for p in in_peers] + [p * inner + my_in for p in out_peers],
+    )
+    first, second = [], []
+    for j, (i, start, size) in enumerate(jobs):
+        cols = pl.ds(start, size)
+        first.append(
+            [
+                send(
+                    ins[i].at[:, peer, :, cols],
+                    recv1[i].at[d, :, :, cols],
+                    send1_sem.at[j * (inner - 1) + d],
+                    recv1_sem.at[j * (inner - 1) + d],
+                    axis,
+                    my_out * inner + peer,
+                )
+                for d, peer in enumerate(in_peers)
+            ]
+        )
+    for j, (i, start, size) in enumerate(jobs):
+        cols = pl.ds(start, size)
+        for copy in first[j]:
+            copy.wait_recv()
+        if inner > 1:
+            for z in range(outer):
+                total = ins[i][z, my_in, :, cols].astype(f32)
+                for d in range(inner - 1):
+                    total = total + recv1[i][d, z, :, cols].astype(f32)
+                mid[i][z, :, cols] = total.astype(mid[i].dtype)
+        second.append(
+            [
+                send(
+                    mid[i].at[peer, :, cols] if inner > 1 else ins[i].at[peer, 0, :, cols],
+                    recv2[i].at[d, :, cols],
+                    send2_sem.at[j * (outer - 1) + d],
+                    recv2_sem.at[j * (outer - 1) + d],
+                    axis,
+                    peer * inner + my_in,
+                )
+                for d, peer in enumerate(out_peers)
+            ]
+        )
+    for j, (i, start, size) in enumerate(jobs):
+        cols = pl.ds(start, size)
+        for copy in second[j]:
+            copy.wait_recv()
+        own = mid[i][my_out, :, cols] if inner > 1 else ins[i][my_out, 0, :, cols]
+        total = own.astype(f32)
+        for d in range(outer - 1):
+            total = total + recv2[i][d, :, cols].astype(f32)
+        outs[i][:, cols] = total
+    for copies in first + second:
+        for copy in copies:
+            copy.wait_send()
+
+
+def pieces(columns, most):
+    tiles = columns // 128
+    if columns % 128 or tiles == 0:
+        return [(0, columns)]
+    most = min(most, tiles)
+    edges = [128 * (tiles * p // most) for p in range(most + 1)]
+    return [(lo, hi - lo) for lo, hi in zip(edges, edges[1:])]
+
+
+VMEM = pl.BlockSpec(memory_space=pltpu.VMEM)
+LIMIT = 56 * 1024 * 1024
+
+
+def scatter_sum(arrays, axis, outer, inner, most, ident):
+    count = len(arrays)
+    shapes = [a.shape[1:] for a in arrays]
+    arrays = [a.reshape(outer, inner, *a.shape[1:]) for a in arrays]
+    jobs = [(i, s, n) for i, (_, c) in enumerate(shapes) for s, n in pieces(c, most)]
+    scratch = []
+    if inner > 1:
+        scratch += [pltpu.VMEM((inner - 1, outer, *s), a.dtype) for s, a in zip(shapes, arrays)]
+        scratch += [pltpu.VMEM((outer, *s), a.dtype) for s, a in zip(shapes, arrays)]
+    scratch += [pltpu.VMEM((outer - 1, *s), a.dtype) for s, a in zip(shapes, arrays)]
+    if inner > 1:
+        scratch += [pltpu.SemaphoreType.DMA((len(jobs) * (inner - 1),))] * 2
+    scratch += [pltpu.SemaphoreType.DMA((len(jobs) * (outer - 1),))] * 2
+    return pl.pallas_call(
+        functools.partial(scatter_kernel, axis, outer, inner, jobs, count),
+        out_shape=[jax.ShapeDtypeStruct(s, jnp.float32) for s in shapes],
+        in_specs=[VMEM] * count,
+        out_specs=[VMEM] * count,
+        scratch_shapes=scratch,
+        compiler_params=pltpu.CompilerParams(
+            collective_id=ident, has_side_effects=True, vmem_limit_bytes=LIMIT
+        ),
+    )(*arrays)
+
+
+def gather_kernel(axis, outer, inner, parts, x_ref, out_ref, *sems):
+    out_send, out_recv = sems[:2]
+    if inner > 1:
+        in_send, in_recv = sems[2:4]
+    own_sem = sems[-1]
+    me = lax.axis_index(axis)
+    my_out, my_in = lax.div(me, inner), lax.rem(me, inner)
+    in_peers = [flip(my_in, d) for d in range(1, inner)]
+    out_peers = [flip(my_out, d) for d in range(1, outer)]
+    meet(
+        axis,
+        [my_out * inner + p for p in in_peers] + [p * inner + my_in for p in out_peers],
+    )
+    own = pltpu.make_async_copy(x_ref, out_ref.at[me], own_sem)
+    own.start()
+    across, along = [], []
+
+    def pass_on(block, src, c, e):
+        cols = pl.ds(*parts[c])
+        for d, peer in enumerate(in_peers):
+            k = (c * outer + e) * (inner - 1) + d
+            along.append(
+                send(
+                    src,
+                    out_ref.at[block, :, cols],
+                    in_send.at[k],
+                    in_recv.at[k],
+                    axis,
+                    my_out * inner + peer,
+                )
+            )
+
+    for c, part in enumerate(parts):
+        cols = pl.ds(*part)
+        across.append(
+            [
+                send(
+                    x_ref.at[:, cols],
+                    out_ref.at[me, :, cols],
+                    out_send.at[c * (outer - 1) + d],
+                    out_recv.at[c * (outer - 1) + d],
+                    axis,
+                    peer * inner + my_in,
+                )
+                for d, peer in enumerate(out_peers)
+            ]
+        )
+        pass_on(me, x_ref.at[:, cols], c, 0)
+    for c, part in enumerate(parts):
+        for d, peer in enumerate(out_peers):
+            across[c][d].wait_recv()
+            block = peer * inner + my_in
+            pass_on(block, out_ref.at[block, :, pl.ds(*part)], c, d + 1)
+    own.wait()
+    for copy in along:
+        copy.wait_recv()
+    for copies in across + [along]:
+        for copy in copies:
+            copy.wait_send()
+
+
+def gather(x, axis, outer, inner, most, ident):
+    parts = pieces(x.shape[1], most)
+    sems = [pltpu.SemaphoreType.DMA((len(parts) * (outer - 1),))] * 2
+    if inner > 1:
+        sems += [pltpu.SemaphoreType.DMA((len(parts) * outer * (inner - 1),))] * 2
+    sems += [pltpu.SemaphoreType.DMA]
+    return pl.pallas_call(
+        functools.partial(gather_kernel, axis, outer, inner, parts),
+        out_shape=jax.ShapeDtypeStruct((outer * inner, *x.shape), x.dtype),
+        in_specs=[VMEM],
+        out_specs=VMEM,
+        scratch_shapes=sems,
+        compiler_params=pltpu.CompilerParams(
+            collective_id=ident, has_side_effects=True, vmem_limit_bytes=LIMIT
+        ),
+    )(x)
+
+
+def middle_kernel(axis, n, part_ref, tok_ref, out_ref, recv, mine, *sems):
+    f32 = jnp.float32
+    send1, recv1, send2, recv2 = sems
+    me = lax.axis_index(axis)
+    peers = [flip(me, d) for d in range(1, n)]
+    meet(axis, peers)
+    first = [
+        send(part_ref.at[peer], recv.at[d], send1.at[d], recv1.at[d], axis, peer)
+        for d, peer in enumerate(peers)
+    ]
+    for copy in first:
+        copy.wait_recv()
+    total = part_ref[me].astype(f32)
+    for d in range(n - 1):
+        total = total + recv[d].astype(f32)
+    mid = (tok_ref[...].astype(f32) + total).astype(out_ref.dtype)
+    mine[...] = mid
+    second = [
+        send(mine, out_ref.at[me], send2.at[d], recv2.at[d], axis, peer)
+        for d, peer in enumerate(peers)
+    ]
+    out_ref[me] = mid
+    for copy in second:
+        copy.wait_recv()
+    for copy in first + second:
+        copy.wait_send()
+
+
+def middle_sum(partials, tokens, axis, ident):
+    n = partials.shape[0]
+    return pl.pallas_call(
+        functools.partial(middle_kernel, axis, n),
+        out_shape=jax.ShapeDtypeStruct(partials.shape, tokens.dtype),
+        in_specs=[VMEM] * 2,
+        out_specs=VMEM,
+        scratch_shapes=[
+            pltpu.VMEM((n - 1, *partials.shape[1:]), partials.dtype),
+            pltpu.VMEM(partials.shape[1:], tokens.dtype),
+        ]
+        + [pltpu.SemaphoreType.DMA((n - 1,))] * 4,
+        compiler_params=pltpu.CompilerParams(
+            collective_id=ident, has_side_effects=True, vmem_limit_bytes=LIMIT
+        ),
+    )(partials, tokens)
+
 
 D = 4096
 
@@ -46,6 +318,8 @@
 
 
 def per_device(
+    n_kv,
+    n_tp,
     tokens,
     norm_gain,
     w_query,
@@ -78,7 +352,20 @@
     head_dim = tail_keys.shape[3]
     seq_dev = lengths.shape[0]
     width = heads * head_dim
-    wide = lax.all_gather(tokens, "tp", axis=1, tiled=True)
+    inner = n_kv // 4 if n_kv % 4 == 0 else 1
+    outer = n_kv // inner
+    seqs, own_cols = tokens.shape
+
+    def join(blocks):
+        return jnp.moveaxis(blocks, 0, 1).reshape(seqs, n_tp * own_cols)
+
+    def split(whole):
+        return jnp.moveaxis(whole.reshape(seqs, n_tp, own_cols), 1, 0)
+
+    def by_owner(array):
+        return array.reshape(n_kv, seq_dev, array.shape[1])
+
+    wide = join(gather(tokens, "tp", n_tp, 1, 1, 0))
     widef = wide.astype(f32)
     scaled = (widef * norm_gain).astype(bf)
 
@@ -89,15 +376,16 @@
     joined = jnp.concatenate([w_query, w_key, w_value, w_outgate], axis=1)
     proj = jnp.dot(scaled, joined, preferred_element_type=f32)
     gates = jnp.dot(scaled, gate_weights, preferred_element_type=f32)
-    tokf = tokens.astype(f32)
-    sq_all = lax.psum(jnp.sum(tokf * tokf, axis=1), ("kv", "tp"))
-    proj, gates = (
-        lax.psum_scatter(proj, "kv", scatter_dimension=0, tiled=True),
-        lax.psum_scatter(gates, "kv", scatter_dimension=0, tiled=True),
-    )
-    inv_first = lax.dynamic_slice_in_dim(lax.rsqrt(sq_all / D + EPS), kv_pos * seq_dev, seq_dev)
-    proj = proj * inv_first[:, None]
-    gates = gates * inv_first[:, None]
+    part_sq1 = jnp.sum(widef * widef, axis=1, keepdims=True)
+    gates = jnp.concatenate(
+        [gates, part_sq1, jnp.zeros((seqs, 127 - 2 * heads), f32)], axis=1
+    )
+    gates, proj = scatter_sum(
+        [by_owner(gates), by_owner(proj.astype(bf))], "kv", outer, inner, 6, 1
+    )
+    inv_first = lax.rsqrt(gates[:, 2 * heads : 2 * heads + 1] / D + EPS)
+    proj = proj * inv_first
+    gates = gates[:, : 2 * heads] * inv_first
     query = proj[:, :width].reshape(seq_dev, heads, head_dim)
     key = proj[:, width : 2 * width].reshape(seq_dev, heads, head_dim) * head_dim ** (-0.5)
     value = proj[:, 2 * width : 3 * width].reshape(seq_dev, heads, head_dim)
@@ -120,37 +408,36 @@
     )
     normed = recalled * lax.rsqrt(jnp.mean(recalled * recalled, axis=2, keepdims=True) + EPS)
     mixed = (normed.reshape(seq_dev, width) * head_gain * jax.nn.sigmoid(outgate)).astype(bf)
-    partial_value = jnp.dot(
-        lax.all_gather(mixed, "kv", axis=0, tiled=True), w_proj, preferred_element_type=f32
-    )
-    attended = lax.psum(partial_value.astype(jnp.bfloat16), "tp").astype(jnp.float32)
-    middle = (widef + attended).astype(bf)
+    all_mixed = gather(mixed, "kv", outer, inner, 1, 2).reshape(seqs, width)
+    partial_value = jnp.dot(all_mixed, w_proj, preferred_element_type=f32)
+    middle = join(middle_sum(split(partial_value.astype(bf)), tokens, "tp", 3))
     middlef = middle.astype(f32)
     part_sq2 = jnp.sum(middlef * middlef, axis=1)
     scaled_mid = (middlef * mixer_gain).astype(bf)
     gate_part = jnp.dot(scaled_mid, w_gate, preferred_element_type=f32)
     up_part = jnp.dot(scaled_mid, w_up, preferred_element_type=f32)
-    gate_sh, up_sh, sq_sh = (
-        lax.psum_scatter(gate_part, "kv", scatter_dimension=0, tiled=True),
-        lax.psum_scatter(up_part, "kv", scatter_dimension=0, tiled=True),
-        lax.psum_scatter(part_sq2, "kv", scatter_dimension=0, tiled=True),
-    )
+    sq_wide = jnp.broadcast_to(part_sq2[:, None], (seqs, 128))
+    sq_sh, gate_sh, up_sh = scatter_sum(
+        [by_owner(sq_wide), by_owner(gate_part.astype(bf)), by_owner(up_part.astype(bf))],
+        "kv",
+        outer,
+        inner,
+        5,
+        4,
+    )
+    sq_sh = sq_sh[:, 0]
     inv_second = lax.rsqrt(sq_sh / D + EPS)[:, None]
     hidden_sh = (jax.nn.silu(gate_sh * inv_second) * (up_sh * inv_second)).astype(bf)
-    down_part = jnp.dot(
-        lax.all_gather(hidden_sh, "kv", axis=0, tiled=True), w_down, preferred_element_type=f32
-    )
-    down_sum = lax.psum_scatter(
-        down_part.astype(jnp.bfloat16), "tp", scatter_dimension=1, tiled=True
-    ).astype(jnp.float32)
-    columns = down_sum.shape[1]
-    residual = lax.dynamic_slice_in_dim(middlef, tp_pos * columns, columns, 1)
+    hidden = gather(hidden_sh, "kv", outer, inner, 4, 5).reshape(seqs, hidden_sh.shape[1])
+    down_part = jnp.dot(hidden, w_down, preferred_element_type=f32)
+    (down_sum,) = scatter_sum([split(down_part.astype(bf))], "tp", n_tp, 1, 1, 6)
+    residual = lax.dynamic_slice_in_dim(middlef, tp_pos * own_cols, own_cols, 1)
     return (residual + down_sum).astype(bf)
 
 
 def solution(mesh):
     return jax.shard_map(
-        per_device,
+        functools.partial(per_device, mesh.shape["kv"], mesh.shape["tp"]),
         mesh=mesh,
         in_specs=(
             P(None, ("kv", "tp")),

time: 530 us -> 248 us (0.47)
  waiting for transfers between devices: 338 us -> 0 us
  Pallas kernels: 0 us -> 172 us
  blocking collectives: 102 us -> 0 us
  between operations: 14.3 us -> 0.33 us
    reduce_scatter x3 -> x0, waiting for transfers between devices: 220 us -> none  [the longest x1 93.3 us: per_device(): lax.psum_scatter(up_part, 'kv', scatter_dimension=0, tiled=True)]
    pallas_call x0 -> x7, Pallas kernels: none -> 172 us  [the longest x3 102 us: scatter_sum(): pl.pallas_call(functools.partial(scatter_kernel, axis, outer, inner, jobs...]
    all_gather x1 -> x0, waiting for transfers between devices: 49.5 us -> none  [per_device(): lax.all_gather(hidden_sh, 'kv', axis=0, tiled=True)]
    psum x1 -> x0, blocking collectives: 40.2 us -> none  [per_device(): sq_all = lax.psum(jnp.sum(tokf * tokf, axis=1), ('kv', 'tp'))]
    all_gather x2 -> x0, blocking collectives: 39.2 us -> none  [the longest x1 31 us: per_device(): lax.all_gather(mixed, 'kv', axis=0, tiled=True)]
    unnamed x9 -> x0, waiting for transfers between devices: 36.4 us -> none
    psum x1 -> x0, waiting for transfers between devices: 32 us -> none  [per_device(): lax.psum(partial_value.astype(jnp.bfloat16), 'tp').astype(jnp.float32)]
    unnamed x1 -> x0, blocking collectives: 22.5 us -> none
  transfers between devices with their start and end apart: 7 -> 0, of which waited for: 7 -> 0; matrix products, arithmetic and copies ran while one was open for 4% -> 0% of each run, Pallas kernels for 0% -> 0%
where the time goes in v1:
time: 248 us; the launch traced here: 247 us
  Pallas kernels  172 us (69%)
  matrix products  33 us (13%)
  local copies, waits for them, and re-layouts  22.4 us (9%)
  other arithmetic  19.5 us (8%)
    pallas_call x3, Pallas kernels, scatter_sum(): pl.pallas_call(functools.partial(scatter_kernel, axis, outer, inner, jobs...  102 us
    pallas_call x3, Pallas kernels, gather(): pl.pallas_call(functools.partial(gather_kernel, axis, outer, inner, parts...  53.9 us
    pallas_call x1, Pallas kernels, middle_sum(): pl.pallas_call(functools.partial(middle_kernel, axis, n), out_shape=jax.S...  15.3 us
    dot_general x1, matrix products, recall(): memory = jnp.einsum('shvk,shk->shv', state_c, query)  8.64 us
    convert_element_type x3, local copies, waits for them, and re-layouts, per_device(): widef = wide.astype(f32)  6.05 us

profile of v1, /device:TPU:0, one launch (start us, length us, event | category | flops | bytes accessed | tf_op | source)
XLA Modules:
  0.0 246.8 jit_solution(14454954142695654002)
XLA Ops:
  0.0 0.9 dynamic_slice.10
  0.9 0.8 dynamic_slice.9
  1.8 10.2 %shard_map.208 = bf16[4,384,128]{2,1,0:T(8,128)(2,1)} custom-call(bf16[384,128]{1,0:T(8,128)(2,1)} %tok_ref.1), custom_call_target="tpu_custom_call" | custom-call | tf_op jit(solution)/shard_map/pallas_call | solution.py:220
  12.0 1.1 convert_bitcast_fusion.1
  13.1 0.9 copy-done.1
  14.0 1.4 copy.51
  15.4 2.3 reshape.92
  17.7 2.0 fusion.10
  19.9 0.2 concatenate.16
  20.2 1.7 maximum_maximum_fusion.refs_0_
  22.0 2.3 copy.54
  24.3 1.3 fusion.9
  25.6 3.7 %convolution_convert_fusion.2 = bf16[384,2048]{1,0:T(8,128)(2,1)} fusion(bf16[384,512]{0,1:T(8,128)(2,1)S(1)} %fusion.9, bf16[512,512]{1,0:T(8,128)(2,1)} %param.27, bf16[512,512]{1,0:T(8,128)(2,1)} %param.26, bf16[512,512]{1,0:T(8,128)(2,1)} %param.25, bf16[512,512]{1,0:T(8,128)(2,1)} %param.24), kind=kOutput, calls=%fused_computation.2 | convolution fusion | flops 814481408 | bytes 4063232 | tf_op jit(solution)/shard_map/dot_general | solution.py:377
  29.3 31.4 %shard_map.209 = (f32[48,128]{1,0:T(8,128)}, f32[48,2048]{1,0:T(8,128)}) custom-call(f32[4,2,48,128]{3,2,1,0:T(8,128)} %maximum_maximum_fusion.refs_0_, bf16[4,2,48,2048]{3,2,1,0:T(8,128)(2,1)} %bitcast.71), custom_call_target="tpu_custom_call" | custom-call | tf_op jit(solution)/shard_map/pallas_call | solution.py:141
  60.8 0.9 rsqrt_reduce_fusion.1
  61.7 0.8 slice_multiply_fusion.1
  63.1 0.6 subtract_exponential_fusion
  63.8 1.1 broadcast_multiply_fusion
  64.9 0.7 slice_multiply_fusion
  65.6 1.6 reshape.96
  67.1 3.7 %fusion.28 = f32[48,4,1,64]{3,2,1,0:T(1,128)S(1)} fusion(f32[48,4,128,1]{2,3,1,0:T(1,128)} %bitcast.78, bf16[48,4,64,128]{3,2,1,0:T(8,128)(2,1)} %param.39), kind=kOutput, calls=%fused_computation.64 | convolution fusion | flops 3145728 | bytes 3293184 | tf_op jit(solution)/shard_map/shpd,shd->shp/dot_general | solution.py:309
  71.1 1.6 fusion.29
  72.6 1.6 reshape.84
  74.2 1.6 mul.164
  75.8 1.1 multiply_reduce_fusion.1
  76.8 1.4 exponential_multiply_fusion
  78.2 8.6 %fusion.27 = f32[48,4,1,128]{3,2,1,0:T(1,128)} fusion(f32[48,4,128,1]{2,3,1,0:T(1,128)} %bitcast.79, f32[48,4,128,128]{3,2,1,0:T(8,128)} %param.37), kind=kOutput, calls=%fused_computation.63 | convolution fusion | flops 6291456 | bytes 12779520 | tf_op jit(solution)/shard_map/shvk,shk->shv/dot_general | solution.py:311
  86.8 1.6 reshape.85
  88.4 1.3 multiply_reduce_fusion
  89.8 0.7 fusion.13.x_ref
  90.5 12.1 %shard_map.210 = bf16[8,48,512]{2,1,0:T(8,128)(2,1)} custom-call(bf16[48,512]{1,0:T(8,128)(2,1)} %fusion.13.x_ref), custom_call_target="tpu_custom_call" | custom-call | tf_op jit(solution)/shard_map/pallas_call | solution.py:220
  102.6 2.3 convolution_convert_fusion.4
  104.9 1.2 copy.60
  106.1 0.9 copy.61
  107.1 15.3 %shard_map.211 = bf16[4,384,128]{2,1,0:T(8,128)(2,1)} custom-call(bf16[4,384,128]{2,1,0:T(8,128)(2,1)} %bitcast.73, bf16[384,128]{1,0:T(8,128)(2,1)} %tok_ref.1), custom_call_target="tpu_custom_call" | custom-call | tf_op jit(solution)/shard_map/pallas_call | solution.py:262
  122.4 4.7 %convolution_convert_fusion.1 = bf16[384,2816]{1,0:T(8,128)(2,1)} fusion(bf16[512,2816]{1,0:T(8,128)(2,1)} %param.34, f32[512]{0:T(512)S(1)} %copy-done.18, bf16[4,384,128]{2,1,0:T(8,128)(2,1)} %shard_map.211), kind=kOutput, calls=%fused_computation.1 | convolution fusion | flops 1108967424 | bytes 5441536 | tf_op jit(solution)/shard_map/dot_general | solution.py:417
  127.1 2.6 %convolution_convert_fusion = bf16[384,2816]{1,0:T(8,128)(2,1)} fusion(bf16[512,2816]{1,0:T(8,128)(2,1)S(1)} %copy-done.16, f32[512]{0:T(512)S(1)} %copy-done.18, bf16[4,384,128]{2,1,0:T(8,128)(2,1)S(1)} %copy-done.2), kind=kOutput, calls=%fused_computation | convolution fusion | flops 1108967424 | bytes 5441536 | tf_op jit(solution)/shard_map/dot_general | solution.py:418
  130.0 0.8 broadcast_in_dim.22.refs_0_
  130.8 62.6 %shard_map.212 = (f32[48,128]{1,0:T(8,128)}, f32[48,2816]{1,0:T(8,128)}, f32[48,2816]{1,0:T(8,128)}) custom-call(f32[4,2,48,128]{3,2,1,0:T(8,128)} %broadcast_in_dim.22.refs_0_, bf16[4,2,48,2816]{3,2,1,0:T(8,128)(2,1)} %bitcast.69, bf16[4,2,48,2816]{3,2,1,0:T(8,128)(2,1)} %bitcast.70), custom_call_target="tpu_custom_call" | custom-call | tf_op jit(solution)/shard_map/pallas_call | solution.py:141
  193.5 1.0 rsqrt_reduce_fusion
  194.5 2.2 multiply_convert_fusion.2.x_ref
  196.6 31.6 %shard_map.213 = bf16[8,48,2816]{2,1,0:T(8,128)(2,1)} custom-call(bf16[48,2816]{1,0:T(8,128)(2,1)} %multiply_convert_fusion.2.x_ref), custom_call_target="tpu_custom_call" | custom-call | tf_op jit(solution)/shard_map/pallas_call | solution.py:220
  228.2 3.6 %convolution_convert_fusion.3 = bf16[384,512]{1,0:T(8,128)(2,1)} fusion(bf16[384,2816]{1,0:T(8,128)(2,1)} %bitcast.68, bf16[2816,512]{1,0:T(8,128)(2,1)S(1)} %copy-done.17), kind=kOutput, calls=%fused_computation.10 | convolution fusion | flops 1107492864 | bytes 5439488 | tf_op jit(solution)/shard_map/dot_general | solution.py:432
  231.8 1.9 copy.63
  233.8 1.9 copy.64
  235.7 8.4 %shard_map.214 = f32[384,128]{1,0:T(8,128)} custom-call(bf16[4,1,384,128]{3,2,1,0:T(8,128)(2,1)} %bitcast.75), custom_call_target="tpu_custom_call" | custom-call | tf_op jit(solution)/shard_map/pallas_call | solution.py:141
  244.1 1.0 copy_bitcast_fusion
  245.1 1.7 add_convert_fusion
  (50 shorter events, 1.4 us)
Async XLA Ops:
  0.0 71.1 %copy-start = (bf16[48,4,64,128]{3,2,1,0:T(8,128)(2,1)S(1)}, bf16[48,4,64,128]{3,2,1,0:T(8,128)(2,1)}, u32[]{:S(2)}) copy-start(bf16[48,4,64,128]{3,2,1,0:T(8,128)(2,1)} %param.40) | copy-start | bytes 9437188
  0.0 17.7 %copy-start.10 = (f32[512]{0:T(512)S(1)}, f32[512]{0:T(512)}, u32[]{:S(2)}) copy-start(f32[512]{0:T(512)} %param.23) | copy-start | bytes 6148
  11.9 7.8 %copy-start.3 = (bf16[4,384,128]{2,1,0:T(8,128)(2,1)S(1)}, bf16[4,384,128]{2,1,0:T(8,128)(2,1)}, u32[]{:S(2)}) copy-start(bf16[4,384,128]{2,1,0:T(8,128)(2,1)} %shard_map.208) | copy-start | bytes 1179652
  13.1 0.9 copy-start.1
  25.5 37.0 %copy-start.12 = (f32[48,4]{0,1:T(4,128)S(1)}, f32[48,4]{0,1:T(4,128)}, u32[]{:S(2)}) copy-start(f32[48,4]{0,1:T(4,128)} %param.42) | copy-start | bytes 2308
  25.6 37.1 %copy-start.13 = (f32[48,4]{0,1:T(4,128)S(1)}, f32[48,4]{0,1:T(4,128)}, u32[]{:S(2)}) copy-start(f32[48,4]{0,1:T(4,128)} %param.38) | copy-start | bytes 2308
  25.6 37.1 %copy-start.14 = (f32[4]{0:T(128)S(1)}, f32[4]{0:T(128)}, u32[]{:S(2)}) copy-start(f32[4]{0:T(128)} %param.30) | copy-start | bytes 52
  25.6 37.2 %copy-start.15 = (s32[48]{0:T(128)S(1)}, s32[48]{0:T(128)}, u32[]{:S(2)}) copy-start(s32[48]{0:T(128)} %param.43) | copy-start | bytes 580
  25.6 37.3 %copy-start.4 = (f32[48,4,64]{2,1,0:T(4,128)S(1)}, f32[48,4,64]{2,1,0:T(4,128)}, u32[]{:S(2)}) copy-start(f32[48,4,64]{2,1,0:T(4,128)} %param.41) | copy-start | bytes 147460
  62.5 1.2 copy-start.6
  62.8 0.9 copy-start.7
  67.1 3.7 %copy-start.5 = (f32[48,4,64]{2,1,0:T(4,128)S(1)}, f32[48,4,64]{2,1,0:T(4,128)}, u32[]{:S(2)}) copy-start(f32[48,4,64]{2,1,0:T(4,128)} %param.41) | copy-start | bytes 147460
  67.1 3.7 %copy-start.8 = (f32[48,4]{1,0:T(8,128)S(1)}, f32[48,4]{1,0:T(8,128)}, u32[]{:S(2)}) copy-start(f32[48,4]{1,0:T(8,128)} %copy-done.7) | copy-start | bytes 2308
  67.1 3.7 %copy-start.9 = (f32[48,4]{1,0:T(8,128)S(1)}, f32[48,4]{1,0:T(8,128)}, u32[]{:S(2)}) copy-start(f32[48,4]{1,0:T(8,128)} %get-tuple-element.18) | copy-start | bytes 2308
  78.2 11.6 %copy-start.11 = (f32[512]{0:T(512)S(1)}, f32[512]{0:T(512)}, u32[]{:S(2)}) copy-start(f32[512]{0:T(512)} %param.31) | copy-start | bytes 6148
  86.8 35.5 %copy-start.18 = (f32[512]{0:T(512)S(1)}, f32[512]{0:T(512)}, u32[]{:S(2)}) copy-start(f32[512]{0:T(512)} %param.33) | copy-start | bytes 6148
  122.3 4.8 %copy-start.2 = (bf16[4,384,128]{2,1,0:T(8,128)(2,1)S(1)}, bf16[4,384,128]{2,1,0:T(8,128)(2,1)}, u32[]{:S(2)}) copy-start(bf16[4,384,128]{2,1,0:T(8,128)(2,1)} %shard_map.211) | copy-start | bytes 1179652
  122.3 4.8 %copy-start.16 = (bf16[512,2816]{1,0:T(8,128)(2,1)S(1)}, bf16[512,2816]{1,0:T(8,128)(2,1)}, u32[]{:S(2)}) copy-start(bf16[512,2816]{1,0:T(8,128)(2,1)} %param.35) | copy-start | bytes 8650756
  193.4 34.7 %copy-start.17 = (bf16[2816,512]{1,0:T(8,128)(2,1)S(1)}, bf16[2816,512]{1,0:T(8,128)(2,1)}, u32[]{:S(2)}) copy-start(bf16[2816,512]{1,0:T(8,128)(2,1)} %param.36) | copy-start | bytes 8650756
